TPU v7x, 32 devices: a whole 2x2x4 slice. The times are simulated.
32 devices in a mesh: grp: 2 (over x), ep: 16 (over z, y, core).
Axes of the slice: x: 2, y: 2, z: 4, core: 2. Of those that a mesh axis runs over, the one named last changes fastest.
Arguments:
- tokens: bfloat16 [128, 2048], P(('grp', 'ep')), parts along dimension 0, may hold values from -30 to 30
- state: float32 [128, 16, 128, 128], P(('grp', 'ep')), parts along dimension 0, may hold values from -6 to 6
- route_ids: int32 [128, 2], P(('grp', 'ep')), parts along dimension 0, may hold values from 0 to 3, all different within a row; in each aligned block of 4 rows (0 to 3, 4 to 7, ...) at most 3 rows name the same one
- route_weights: bfloat16 [128, 2], P(('grp', 'ep')), parts along dimension 0, may hold values from 0.099609375 to 1
- norm_mix: float32 [2048], replicated, may hold values from 0.1 to 1.9
- w_query: bfloat16 [2048, 2048], P(None, 'ep'), may hold values from -0.125 to 0.125
- w_forget: bfloat16 [2048, 2048], P(None, 'ep'), may hold values from -0.125 to 0.125
- w_input: bfloat16 [2048, 2048], P(None, 'ep'), may hold values from -0.125 to 0.125
- w_gate: bfloat16 [2048, 2048], P(None, 'ep'), may hold values from -0.125 to 0.125
- lower_bound: float32 [2048], replicated, may hold values from 0.05 to 0.9
- head_gain: float32 [128], replicated, may hold values from 0.1 to 1.9
- w_out: bfloat16 [2048, 2048], P(None, 'ep'), may hold values from -0.125 to 0.125
- norm_ffn: float32 [2048], replicated, may hold values from 0.1 to 1.9
- expert_gate: bfloat16 [2048, 28672], P(None, 'ep'), may hold values from -0.125 to 0.125
- expert_up: bfloat16 [2048, 28672], P(None, 'ep'), may hold values from -0.125 to 0.125
- expert_down: bfloat16 [28672, 2048], P('ep'), may hold values from -0.0625 to 0.0625
Outputs:
- layer_out: bfloat16 [128, 2048], P(('grp', 'ep')), parts along dimension 0
- new_state: float32 [128, 16, 128, 128], P(('grp', 'ep')), parts along dimension 0
There are 2 independent parts, one for each index of `grp`. A program takes and returns all parts, laid end to end along the dimension named above; an argument that names none is the same for every part. Nothing has to cross between parts.
Inputs may be any that keep to these rules, and one draw needn't show every extreme that they name: `route_ids`: each row names 2 different experts; the rows of one device name no expert more than 3 times, and some device names one exactly 3 times.
All inputs are finite; a program needn't handle non-finite values.
Results may differ from a plain program's by a relative error of at most 0.008.
Values may be sent and summed in bfloat16 or wider, within the bound.
No kernel may reach another device: no remote copies, remote signals or barrier semaphores. Data moves between devices by JAX's collectives and lax.ppermute only.
A program may use at most 64 MiB of HBM per device.

v0:
```python
import jax
import jax.numpy as jnp
from jax import lax
from jax.sharding import PartitionSpec as P

FF = 7168
EXPERTS = 4
CAP = 3
epsilon = 1e-06


def rms_scale(values, gain):
    return values * lax.rsqrt(jnp.mean(values * values, axis=-1, keepdims=True) + epsilon) * gain


def mixer_state(projected, state, lower_bound, head_gain):
    query_raw = projected[0].astype(jnp.float32)
    forget_raw = projected[1].astype(jnp.float32)
    input_raw = projected[2].astype(jnp.float32)
    gate_raw = projected[3].astype(jnp.float32)
    seq_rows = state.shape[0]
    heads = state.shape[1]
    head_dim = state.shape[2]
    head_shape = (seq_rows, heads, head_dim)
    log_forget = jnp.logaddexp(
        jnp.log(lower_bound), jnp.log1p(-lower_bound) + jax.nn.log_sigmoid(forget_raw)
    )
    key_vec = (1.0 - lower_bound) * jax.nn.sigmoid(-forget_raw)
    query_vec = jax.nn.silu(query_raw) * head_dim ** (-0.5)
    new_state = (
        jnp.exp(log_forget).reshape(head_shape)[..., None] * state
        + key_vec.reshape(head_shape)[..., None] * input_raw.reshape(head_shape)[:, :, None, :]
    )
    read_out = jnp.einsum(
        "thk,thkv->thv", query_vec.reshape(head_shape), new_state, precision=lax.Precision.HIGHEST
    )
    mixed = rms_scale(read_out, head_gain) * jax.nn.silu(gate_raw.reshape(head_shape))
    return (mixed.reshape(seq_rows, heads * head_dim).astype(jnp.bfloat16), new_state)


def local(
    tokens,
    state,
    route_ids,
    route_weights,
    norm_mix,
    w_query,
    w_forget,
    w_input,
    w_gate,
    lower_bound,
    head_gain,
    w_out,
    norm_ffn,
    expert_gate,
    expert_up,
    expert_down,
):
    model_width = tokens.shape[1]
    expert_group = FF // expert_gate.shape[1]
    all_tokens, all_ids, all_weights = (
        lax.all_gather(tokens, "ep", axis=0, tiled=True),
        lax.all_gather(route_ids, "ep", axis=0, tiled=True),
        lax.all_gather(route_weights, "ep", axis=0, tiled=True),
    )
    normed = rms_scale(all_tokens.astype(jnp.float32), norm_mix).astype(jnp.bfloat16)
    projected = jnp.stack(
        [
            jnp.dot(normed, weight, preferred_element_type=jnp.float32).astype(jnp.bfloat16)
            for weight in (w_query, w_forget, w_input, w_gate)
        ]
    )
    owned = lax.all_to_all(projected, "ep", split_axis=1, concat_axis=2, tiled=True)
    mixed, new_state = mixer_state(owned, state, lower_bound, head_gain)
    mixer_cols = jnp.dot(
        lax.all_gather(mixed, "ep", axis=0, tiled=True), w_out, preferred_element_type=jnp.float32
    ).astype(jnp.bfloat16)
    mixer_rows = lax.all_to_all(mixer_cols, "ep", split_axis=0, concat_axis=1, tiled=True)
    middle = tokens.astype(jnp.float32) + mixer_rows.astype(jnp.float32)
    normed_two = rms_scale(middle, norm_ffn).astype(jnp.bfloat16)
    matches = (route_ids[:, :, None] == jnp.arange(EXPERTS, dtype=jnp.int32)[None, None, :]).astype(
        jnp.int32
    )
    hit_mask = jnp.sum(matches, axis=1)
    combined = jnp.sum(
        route_weights.astype(jnp.float32)[:, :, None] * matches.astype(jnp.float32), axis=1
    )
    slot_rank = jnp.cumsum(hit_mask, axis=0) - hit_mask
    slot_ids = jnp.arange(CAP, dtype=jnp.int32)
    placing = (
        (slot_rank.T[:, None, :] == slot_ids[None, :, None]) & (hit_mask.T[:, None, :] > 0)
    ).astype(jnp.float32)
    outgoing = jnp.einsum(
        "ect,td->ecd", placing.astype(jnp.bfloat16), normed_two, preferred_element_type=jnp.float32
    ).astype(jnp.bfloat16)
    outgoing = jnp.repeat(outgoing, expert_group, axis=0)
    arrived = lax.all_to_all(outgoing, "ep", split_axis=0, concat_axis=0, tiled=True)
    gate_act = jnp.einsum("scd,df->scf", arrived, expert_gate, preferred_element_type=jnp.float32)
    up_act = jnp.einsum("scd,df->scf", arrived, expert_up, preferred_element_type=jnp.float32)
    hidden = (jax.nn.silu(gate_act) * up_act).astype(jnp.bfloat16)
    partial_rows = jnp.einsum(
        "scf,fd->scd", hidden, expert_down, preferred_element_type=jnp.float32
    )
    returned = lax.all_to_all(
        partial_rows.astype(jnp.bfloat16), "ep", split_axis=0, concat_axis=0, tiled=True
    ).astype(partial_rows.dtype)
    summed = jnp.sum(
        returned.reshape(EXPERTS, expert_group, returned.shape[1], model_width), axis=1
    )
    expert_total = jnp.einsum(
        "ect,ecd->td", placing * combined.T[:, None, :], summed, precision=lax.Precision.HIGHEST
    )
    layer_out = (middle + expert_total).astype(jnp.bfloat16)
    return (layer_out, new_state)


def solution(mesh):
    return jax.shard_map(
        local,
        mesh=mesh,
        in_specs=(
            P(("grp", "ep"), None),
            P(("grp", "ep"), None, None, None),
            P(("grp", "ep"), None),
            P(("grp", "ep"), None),
            P(),
            P(None, "ep"),
            P(None, "ep"),
            P(None, "ep"),
            P(None, "ep"),
            P(),
            P(),
            P(None, "ep"),
            P(),
            P(None, "ep"),
            P(None, "ep"),
            P("ep", None),
        ),
        out_specs=(P(("grp", "ep"), None), P(("grp", "ep"), None, None, None)),
        check_vma=False,
    )
```

profile of v0, /device:TPU:0, one launch (start us, length us, event | category | flops | bytes accessed | tf_op | source)
XLA Modules:
  0.0 121.8 jit_solution(15939425539012757206)
XLA Ops:
  0.6 24.2 %all-gather = bf16[16,4,2048]{2,1,0:T(4,128)(2,1)S(1)} all-gather(bf16[1,4,2048]{2,1,0:T(4,128)(2,1)} %bitcast.138), channel_id=1, replica_groups=mesh['grp'=2,'ep'=16] {'ep'}, dimensions={0}, use_global_device_ids=true | all-gather | bytes 278528 | tf_op jit(solution)/shard_map/all_gather | solution.py:62
  24.9 0.1 multiply_reduce_fusion
  25.0 0.8 multiply_convert_fusion
  25.9 0.2 fusion.17
  26.1 1.3 %fusion.18 = bf16[1,64,128]{2,1,0:T(8,128)(2,1)S(1)} fusion(bf16[64,2048]{1,0:T(8,128)(2,1)S(1)} %multiply_convert_fusion, bf16[2048,128]{1,0:T(8,128)(2,1)} %param.22), kind=kOutput, calls=%fused_computation.20 | convolution fusion | flops 33562624 | bytes 802816 | tf_op jit(solution)/shard_map/dot_general | solution.py:69
  27.4 1.3 %fusion.19 = bf16[1,64,128]{2,1,0:T(8,128)(2,1)S(1)} fusion(bf16[64,2048]{1,0:T(8,128)(2,1)S(1)} %multiply_convert_fusion, bf16[2048,128]{1,0:T(8,128)(2,1)} %param.23), kind=kOutput, calls=%fused_computation.21 | convolution fusion | flops 33562624 | bytes 802816 | tf_op jit(solution)/shard_map/dot_general | solution.py:69
  28.7 1.3 %fusion.20 = bf16[1,64,128]{2,1,0:T(8,128)(2,1)S(1)} fusion(bf16[64,2048]{1,0:T(8,128)(2,1)S(1)} %multiply_convert_fusion, bf16[2048,128]{1,0:T(8,128)(2,1)} %param.24), kind=kOutput, calls=%fused_computation.22 | convolution fusion | flops 33562624 | bytes 802816 | tf_op jit(solution)/shard_map/dot_general | solution.py:69
  30.0 0.7 copy.66
  30.7 3.5 %all-to-all-start = ((bf16[4,64,128]{2,0,1:T(4,128)(2,1)}), bf16[4,64,128]{2,0,1:T(4,128)(2,1)S(1)}, u32[]{:S(2)}, u32[]{:S(2)}) async-start(bf16[4,64,128]{2,0,1:T(4,128)(2,1)} %copy.66), calls=%async_computation | async-start | bytes 131072 | tf_op jit(solution)/shard_map/all_to_all | solution.py:73
  34.2 0.7 log_bitcast_fusion
  34.9 0.8 convert_reduce_fusion.1
  35.7 5.3 %all-to-all-done = bf16[4,64,128]{2,0,1:T(4,128)(2,1)S(1)} async-done(((bf16[4,64,128]{2,0,1:T(4,128)(2,1)}), bf16[4,64,128]{2,0,1:T(4,128)(2,1)S(1)}, u32[]{:S(2)}, u32[]{:S(2)}) %all-to-all-start) | async-done | bytes 65568 | tf_op jit(solution)/shard_map/all_to_all | solution.py:73
  41.2 4.4 %multiply_add_fusion = f32[4,16,128,128]{3,2,1,0:T(8,128)S(1)} fusion(f32[4,16,128,128]{3,2,1,0:T(8,128)} %param.17, f32[4,16,128]{2,1,0:T(8,128)S(1)} %fusion.57, f32[4,16,128]{2,1,0:T(8,128)S(1)} %get-tuple-element.3, f32[4,16,128]{2,1,0:T(8,128)S(1)} %get-tuple-element.2), kind=kLoop, calls=%fused_computation.6 | loop fusion | flops 3145728 | bytes 8486912 | tf_op jit(solution)/shard_map/add | solution.py:31
  45.6 2.0 %copy-done.1 = f32[4,16,128,128]{3,2,1,0:T(8,128)} copy-done((f32[4,16,128,128]{3,2,1,0:T(8,128)}, f32[4,16,128,128]{3,2,1,0:T(8,128)S(1)}, u32[]{:S(2)}) %copy-start.1) | copy-done | bytes 4194328
  47.6 3.6 %fusion.73 = f32[4,16,1,128]{3,2,1,0:T(1,128)S(1)} fusion(f32[4,16,128,1]{2,3,1,0:T(1,128)S(1)} %bitcast.137, f32[4,16,128,128]{3,2,1,0:T(8,128)S(1)} %multiply_add_fusion), kind=kOutput, calls=%fused_computation.103 | convolution fusion | flops 12582912 | bytes 4259840 | tf_op jit(solution)/shard_map/thk,thkv->thv/dot_general | solution.py:34
  51.3 0.1 multiply_reduce_fusion.2
  51.5 18.4 %all-gather.1 = bf16[16,4,2048]{2,1,0:T(4,128)(2,1)S(1)} all-gather(bf16[1,4,2048]{2,1,0:T(4,128)(2,1)S(1)} %reshape.164), channel_id=1, replica_groups=mesh['grp'=2,'ep'=16] {'ep'}, dimensions={0}, use_global_device_ids=true | all-gather | bytes 278528 | tf_op jit(solution)/shard_map/all_gather | solution.py:76
  70.0 0.8 convolution_convert_fusion.1
  70.8 3.5 %all-to-all-start.1 = ((bf16[16,4,128]{2,1,0:T(4,128)(2,1)}), bf16[16,4,128]{2,1,0:T(4,128)(2,1)S(1)}, u32[]{:S(2)}, u32[]{:S(2)}) async-start(bf16[16,4,128]{2,1,0:T(4,128)(2,1)} %bitcast.21), calls=%async_computation.1 | async-start | bytes 32768 | tf_op jit(solution)/shard_map/all_to_all | solution.py:78
  74.3 6.5 %all-to-all-done.1 = bf16[16,4,128]{2,1,0:T(4,128)(2,1)S(1)} async-done(((bf16[16,4,128]{2,1,0:T(4,128)(2,1)}), bf16[16,4,128]{2,1,0:T(4,128)(2,1)S(1)}, u32[]{:S(2)}, u32[]{:S(2)}) %all-to-all-start.1) | async-done | bytes 16416 | tf_op jit(solution)/shard_map/all_to_all | solution.py:78
  80.8 0.1 multiply_reduce_fusion.1
  80.9 0.2 convolution_convert_fusion
  81.2 0.1 broadcast_in_dim.2
  81.3 12.6 %all_to_all.38 = bf16[16,3,2048]{2,1,0:T(4,128)(2,1)S(1)} all-to-all(bf16[16,3,2048]{2,1,0:T(4,128)(2,1)S(1)} %bitcast.130), channel_id=1, replica_groups=mesh['grp'=2,'ep'=16] {'ep'}, dimensions={0} | all-to-all | bytes 393216 | tf_op jit(solution)/shard_map/all_to_all | solution.py:97
  93.9 4.5 %fusion.4 = f32[16,3,1792]{2,0,1:T(8,128)S(1)} fusion(bf16[2048,1792]{1,0:T(8,128)(2,1)} %param.29, bf16[16,3,2048]{2,1,0:T(4,128)(2,1)S(1)} %all_to_all.38), kind=kOutput, calls=%fused_computation.4 | convolution fusion | flops 352321536 | bytes 7880704 | tf_op jit(solution)/shard_map/scd,df->scf/dot_general | solution.py:98
  98.5 7.9 %fusion.12 = bf16[16,3,2048]{2,0,1:T(8,128)(2,1)S(1)} fusion(bf16[1792,2048]{1,0:T(8,128)(2,1)} %param.31, bf16[2048,1792]{1,0:T(8,128)(2,1)} %param.30, f32[16,3,1792]{2,0,1:T(8,128)S(1)} %fusion.4, bf16[16,3,2048]{2,1,0:T(4,128)(2,1)S(1)} %all_to_all.38), kind=kOutput, calls=%fused_computation.9 | convolution fusion | flops 705257472 | bytes 15417344 | tf_op jit(solution)/shard_map/scf,fd->scd/dot_general | solution.py:101
  106.4 0.9 copy.73
  107.2 3.5 %all-to-all-start.3 = ((bf16[16,3,2048]{2,1,0:T(4,128)(2,1)}), bf16[16,3,2048]{2,1,0:T(4,128)(2,1)S(1)}, u32[]{:S(2)}, u32[]{:S(2)}) async-start(bf16[16,3,2048]{2,1,0:T(4,128)(2,1)} %copy.73), calls=%async_computation.3 | async-start | bytes 524288 | tf_op jit(solution)/shard_map/all_to_all | solution.py:104
  110.8 0.1 fusion.63
  110.9 9.9 %all-to-all-done.3 = bf16[16,3,2048]{2,1,0:T(4,128)(2,1)S(1)} async-done(((bf16[16,3,2048]{2,1,0:T(4,128)(2,1)}), bf16[16,3,2048]{2,1,0:T(4,128)(2,1)S(1)}, u32[]{:S(2)}, u32[]{:S(2)}) %all-to-all-start.3) | async-done | bytes 196640 | tf_op jit(solution)/shard_map/all_to_all | solution.py:104
  120.7 0.1 convert_reduce_fusion
  120.9 0.9 fusion.16
  (31 shorter events, 0.5 us)
Async XLA Ops:
  0.6 25.2 %copy-start = (bf16[2048,128]{1,0:T(8,128)(2,1)S(1)}, bf16[2048,128]{1,0:T(8,128)(2,1)}, u32[]{:S(2)}) copy-start(bf16[2048,128]{1,0:T(8,128)(2,1)} %param.21) | copy-start | bytes 1572868
  28.7 22.7 %copy-start.5 = (f32[128]{0:T(128)S(1)}, f32[128]{0:T(128)}, u32[]{:S(2)}) copy-start(f32[128]{0:T(128)} %param.26) | copy-start | bytes 1540
  30.0 40.0 %copy-start.2 = (bf16[2048,128]{1,0:T(8,128)(2,1)S(1)}, bf16[2048,128]{1,0:T(8,128)(2,1)}, u32[]{:S(2)}) copy-start(bf16[2048,128]{1,0:T(8,128)(2,1)} %param.27) | copy-start | bytes 1572868
  30.7 10.4 %all-to-all-start = ((bf16[4,64,128]{2,0,1:T(4,128)(2,1)}), bf16[4,64,128]{2,0,1:T(4,128)(2,1)S(1)}, u32[]{:S(2)}, u32[]{:S(2)}) async-start(bf16[4,64,128]{2,0,1:T(4,128)(2,1)} %copy.66), calls=%async_computation | async-start | bytes 131072 | tf_op jit(solution)/shard_map/all_to_all | solution.py:73
  41.1 39.7 %copy-start.3 = (bf16[4,2048]{1,0:T(4,128)(2,1)S(1)}, bf16[4,2048]{1,0:T(4,128)(2,1)}, u32[]{:S(2)}) copy-start(bf16[4,2048]{1,0:T(4,128)(2,1)} %param.16) | copy-start | bytes 49156
  41.1 39.8 %copy-start.6 = (f32[2048]{0:T(1024)S(1)}, f32[2048]{0:T(1024)}, u32[]{:S(2)}) copy-start(f32[2048]{0:T(1024)} %param.28) | copy-start | bytes 24580
  45.6 2.0 %copy-start.1 = (f32[4,16,128,128]{3,2,1,0:T(8,128)}, f32[4,16,128,128]{3,2,1,0:T(8,128)S(1)}, u32[]{:S(2)}) copy-start(f32[4,16,128,128]{3,2,1,0:T(8,128)S(1)} %multiply_add_fusion) | copy-start | bytes 12582916
  70.8 10.0 %all-to-all-start.1 = ((bf16[16,4,128]{2,1,0:T(4,128)(2,1)}), bf16[16,4,128]{2,1,0:T(4,128)(2,1)S(1)}, u32[]{:S(2)}, u32[]{:S(2)}) async-start(bf16[16,4,128]{2,1,0:T(4,128)(2,1)} %bitcast.21), calls=%async_computation.1 | async-start | bytes 32768 | tf_op jit(solution)/shard_map/all_to_all | solution.py:78
  98.4 12.3 %copy-start.7 = (bf16[4,2]{0,1:T(2,128)(2,1)S(1)}, bf16[4,2]{0,1:T(2,128)(2,1)}, u32[]{:S(2)}) copy-start(bf16[4,2]{0,1:T(2,128)(2,1)} %param.19) | copy-start | bytes 52
  98.5 12.3 %copy-start.4 = (s32[4,2]{0,1:T(2,128)S(1)}, s32[4,2]{0,1:T(2,128)}, u32[]{:S(2)}) copy-start(s32[4,2]{0,1:T(2,128)} %param.18) | copy-start | bytes 100
  107.2 13.5 %all-to-all-start.3 = ((bf16[16,3,2048]{2,1,0:T(4,128)(2,1)}), bf16[16,3,2048]{2,1,0:T(4,128)(2,1)S(1)}, u32[]{:S(2)}, u32[]{:S(2)}) async-start(bf16[16,3,2048]{2,1,0:T(4,128)(2,1)} %copy.73), calls=%async_computation.3 | async-start | bytes 524288 | tf_op jit(solution)/shard_map/all_to_all | solution.py:104
where the time goes:
time: 123 us; the launch traced here: 122 us
  blocking collectives  55.2 us (45%)
  matrix products  22.1 us (18%)
  waiting for transfers between devices  21.7 us (18%)
  starting transfers between devices  10.5 us (9%)
  other arithmetic  7.51 us (6%)
  local copies, waits for them, and re-layouts  3.88 us (3%)
    all_gather x1, blocking collectives, local(): lax.all_gather(tokens, 'ep', axis=0, tiled=True)  24.2 us
    all_gather x1, blocking collectives, local(): lax.all_gather(mixed, 'ep', axis=0, tiled=True)  18.4 us
    all_to_all x1, blocking collectives, local(): lax.all_to_all(outgoing, 'ep', split_axis=0, concat_axis=0, tiled=True)  12.6 us
    all_to_all x1, waiting for transfers between devices, local(): lax.all_to_all(partial_rows.astype(jnp.bfloat16), 'ep', split_axis=0, con...  9.86 us
    dot_general x1, matrix products, local(): jnp.einsum('scf,fd->scd', hidden, expert_down, preferred_element_type=jnp...  7.88 us
    all_to_all x1, waiting for transfers between devices, local(): lax.all_to_all(mixer_cols, 'ep', split_axis=0, concat_axis=1, tiled=True)  6.45 us
    all_to_all x1, waiting for transfers between devices, local(): lax.all_to_all(projected, 'ep', split_axis=1, concat_axis=2, tiled=True)  5.34 us
    dot_general x1, matrix products, local(): jnp.einsum('scd,df->scf', arrived, expert_gate, preferred_element_type=jn...  4.49 us
  transfers between devices with their start and end apart: 3, of which 3 were waited for; matrix products, arithmetic and copies ran while one was open for 1% of the time, Pallas kernels for 0%

commit v1 on v0

--- a/solution.py
+++ b/solution.py
@@ -75,7 +75,10 @@
     mixer_cols = jnp.dot(
         lax.all_gather(mixed, "ep", axis=0, tiled=True), w_out, preferred_element_type=jnp.float32
     ).astype(jnp.bfloat16)
-    mixer_rows = lax.all_to_all(mixer_cols, "ep", split_axis=0, concat_axis=1, tiled=True)
+    devices = lax.axis_size("ep")
+    blocks = jnp.stack(jnp.split(mixer_cols, devices, axis=0), axis=0)
+    blocks = lax.all_to_all(blocks, "ep", split_axis=0, concat_axis=0)
+    mixer_rows = jnp.concatenate(blocks, axis=1)
     middle = tokens.astype(jnp.float32) + mixer_rows.astype(jnp.float32)
     normed_two = rms_scale(middle, norm_ffn).astype(jnp.bfloat16)
     matches = (route_ids[:, :, None] == jnp.arange(EXPERTS, dtype=jnp.int32)[None, None, :]).astype(

time: 123 us -> 131 us (1.065)
  local copies, waits for them, and re-layouts: 3.88 us -> 12.9 us
    unnamed x18 -> x33, local copies, waits for them, and re-layouts: 2.13 us -> 10.6 us
where the time goes in v1:
time: 131 us; the launch traced here: 130 us
  blocking collectives  55.2 us (42%)
  waiting for transfers between devices  21.7 us (17%)
  matrix products  21.5 us (16%)
  local copies, waits for them, and re-layouts  12.9 us (10%)
  starting transfers between devices  10.5 us (8%)
  other arithmetic  7.51 us (6%)
    all_gather x1, blocking collectives, local(): lax.all_gather(tokens, 'ep', axis=0, tiled=True)  24.2 us
    all_gather x1, blocking collectives, local(): lax.all_gather(mixed, 'ep', axis=0, tiled=True)  18.4 us
    all_to_all x1, blocking collectives, local(): lax.all_to_all(outgoing, 'ep', split_axis=0, concat_axis=0, tiled=True)  12.6 us
    unnamed x33, local copies, waits for them, and re-layouts  10.6 us
    all_to_all x1, waiting for transfers between devices, local(): lax.all_to_all(partial_rows.astype(jnp.bfloat16), 'ep', split_axis=0, con...  9.86 us
    dot_general x1, matrix products, local(): jnp.einsum('scf,fd->scd', hidden, expert_down, preferred_element_type=jnp...  7.88 us
    all_to_all x1, waiting for transfers between devices, local(): blocks = lax.all_to_all(blocks, 'ep', split_axis=0, concat_axis=0)  6.45 us
    all_to_all x1, waiting for transfers between devices, local(): lax.all_to_all(projected, 'ep', split_axis=1, concat_axis=2, tiled=True)  5.34 us
  transfers between devices with their start and end apart: 3, of which 3 were waited for; matrix products, arithmetic and copies ran while one was open for 1% of the time, Pallas kernels for 0%

profile of v1, /device:TPU:0, one launch (start us, length us, event | category | flops | bytes accessed | tf_op | source)
XLA Modules:
  0.0 130.2 jit_solution(10254236916201537277)
XLA Ops:
  0.6 24.2 %all-gather = bf16[16,4,2048]{2,1,0:T(4,128)(2,1)S(1)} all-gather(bf16[1,4,2048]{2,1,0:T(4,128)(2,1)} %bitcast.201), channel_id=1, replica_groups=mesh['grp'=2,'ep'=16] {'ep'}, dimensions={0}, use_global_device_ids=true | all-gather | bytes 278528 | tf_op jit(solution)/shard_map/all_gather | solution.py:62
  25.0 0.8 multiply_convert_fusion
  26.1 1.3 fusion.18
  27.4 1.3 fusion.19
  28.7 1.3 fusion.20
  30.0 0.7 copy.66
  30.7 3.5 %all-to-all-start = ((bf16[4,64,128]{2,0,1:T(4,128)(2,1)}), bf16[4,64,128]{2,0,1:T(4,128)(2,1)S(1)}, u32[]{:S(2)}, u32[]{:S(2)}) async-start(bf16[4,64,128]{2,0,1:T(4,128)(2,1)} %copy.66), calls=%async_computation | async-start | bytes 131072 | tf_op jit(solution)/shard_map/all_to_all | solution.py:73
  34.2 0.7 log_bitcast_fusion
  34.9 0.8 convert_reduce_fusion.1
  35.7 5.3 %all-to-all-done = bf16[4,64,128]{2,0,1:T(4,128)(2,1)S(1)} async-done(((bf16[4,64,128]{2,0,1:T(4,128)(2,1)}), bf16[4,64,128]{2,0,1:T(4,128)(2,1)S(1)}, u32[]{:S(2)}, u32[]{:S(2)}) %all-to-all-start) | async-done | bytes 65568 | tf_op jit(solution)/shard_map/all_to_all | solution.py:73
  41.2 4.4 %multiply_add_fusion = f32[4,16,128,128]{3,2,1,0:T(8,128)S(1)} fusion(f32[4,16,128,128]{3,2,1,0:T(8,128)} %param.17, f32[4,16,128]{2,1,0:T(8,128)S(1)} %fusion.57, f32[4,16,128]{2,1,0:T(8,128)S(1)} %get-tuple-element.3, f32[4,16,128]{2,1,0:T(8,128)S(1)} %get-tuple-element.2), kind=kLoop, calls=%fused_computation.6 | loop fusion | flops 3145728 | bytes 8486912 | tf_op jit(solution)/shard_map/add | solution.py:31
  45.6 2.0 %copy-done.1 = f32[4,16,128,128]{3,2,1,0:T(8,128)} copy-done((f32[4,16,128,128]{3,2,1,0:T(8,128)}, f32[4,16,128,128]{3,2,1,0:T(8,128)S(1)}, u32[]{:S(2)}) %copy-start.1) | copy-done | bytes 4194328
  47.6 3.6 %fusion.73 = f32[4,16,1,128]{3,2,1,0:T(1,128)S(1)} fusion(f32[4,16,128,1]{2,3,1,0:T(1,128)S(1)} %bitcast.200, f32[4,16,128,128]{3,2,1,0:T(8,128)S(1)} %multiply_add_fusion), kind=kOutput, calls=%fused_computation.135 | convolution fusion | flops 12582912 | bytes 4259840 | tf_op jit(solution)/shard_map/thk,thkv->thv/dot_general | solution.py:34
  51.5 18.4 %all-gather.1 = bf16[16,4,2048]{2,1,0:T(4,128)(2,1)S(1)} all-gather(bf16[1,4,2048]{2,1,0:T(4,128)(2,1)S(1)} %reshape.163), channel_id=1, replica_groups=mesh['grp'=2,'ep'=16] {'ep'}, dimensions={0}, use_global_device_ids=true | all-gather | bytes 278528 | tf_op jit(solution)/shard_map/all_gather | solution.py:76
  70.2 0.6 constant_dynamic-update-slice_fusion.15
  70.8 0.6 constant_dynamic-update-slice_fusion.14
  71.9 0.6 constant_dynamic-update-slice_fusion.12
  73.0 0.6 constant_dynamic-update-slice_fusion.10
  74.2 0.6 constant_dynamic-update-slice_fusion.8
  75.3 0.6 constant_dynamic-update-slice_fusion.6
  76.4 0.6 constant_dynamic-update-slice_fusion.4
  77.5 0.6 constant_dynamic-update-slice_fusion.2
  78.7 0.6 constant_dynamic-update-slice_fusion
  79.2 3.5 %all-to-all-start.1 = ((bf16[16,4,128]{2,1,0:T(4,128)(2,1)}), bf16[16,4,128]{2,1,0:T(4,128)(2,1)S(1)}, u32[]{:S(2)}, u32[]{:S(2)}) async-start(bf16[16,4,128]{2,1,0:T(4,128)(2,1)} %constant_dynamic-update-slice_fusion), calls=%async_computation.1 | async-start | bytes 32768 | tf_op jit(solution)/shard_map/all_to_all | solution.py:80
  82.8 6.5 %all-to-all-done.1 = bf16[16,4,128]{2,1,0:T(4,128)(2,1)S(1)} async-done(((bf16[16,4,128]{2,1,0:T(4,128)(2,1)}), bf16[16,4,128]{2,1,0:T(4,128)(2,1)S(1)}, u32[]{:S(2)}, u32[]{:S(2)}) %all-to-all-start.1) | async-done | bytes 16416 | tf_op jit(solution)/shard_map/all_to_all | solution.py:80
  89.8 12.6 %all_to_all.30 = bf16[16,3,2048]{2,1,0:T(4,128)(2,1)S(1)} all-to-all(bf16[16,3,2048]{2,1,0:T(4,128)(2,1)S(1)} %bitcast.193), channel_id=1, replica_groups=mesh['grp'=2,'ep'=16] {'ep'}, dimensions={0} | all-to-all | bytes 393216 | tf_op jit(solution)/shard_map/all_to_all | solution.py:100
  102.4 4.5 %fusion.4 = f32[16,3,1792]{2,0,1:T(8,128)S(1)} fusion(bf16[2048,1792]{1,0:T(8,128)(2,1)} %param.29, bf16[16,3,2048]{2,1,0:T(4,128)(2,1)S(1)} %all_to_all.30), kind=kOutput, calls=%fused_computation.4 | convolution fusion | flops 352321536 | bytes 7880704 | tf_op jit(solution)/shard_map/scd,df->scf/dot_general | solution.py:101
  106.9 7.9 %fusion.12 = bf16[16,3,2048]{2,0,1:T(8,128)(2,1)S(1)} fusion(bf16[1792,2048]{1,0:T(8,128)(2,1)} %param.31, bf16[2048,1792]{1,0:T(8,128)(2,1)} %param.30, f32[16,3,1792]{2,0,1:T(8,128)S(1)} %fusion.4, bf16[16,3,2048]{2,1,0:T(4,128)(2,1)S(1)} %all_to_all.30), kind=kOutput, calls=%fused_computation.9 | convolution fusion | flops 705257472 | bytes 15417344 | tf_op jit(solution)/shard_map/scf,fd->scd/dot_general | solution.py:104
  114.8 0.9 copy.73
  115.7 3.5 %all-to-all-start.3 = ((bf16[16,3,2048]{2,1,0:T(4,128)(2,1)}), bf16[16,3,2048]{2,1,0:T(4,128)(2,1)S(1)}, u32[]{:S(2)}, u32[]{:S(2)}) async-start(bf16[16,3,2048]{2,1,0:T(4,128)(2,1)} %copy.73), calls=%async_computation.3 | async-start | bytes 524288 | tf_op jit(solution)/shard_map/all_to_all | solution.py:107
  119.3 9.9 %all-to-all-done.3 = bf16[16,3,2048]{2,1,0:T(4,128)(2,1)S(1)} async-done(((bf16[16,3,2048]{2,1,0:T(4,128)(2,1)}), bf16[16,3,2048]{2,1,0:T(4,128)(2,1)S(1)}, u32[]{:S(2)}, u32[]{:S(2)}) %all-to-all-start.3) | async-done | bytes 196640 | tf_op jit(solution)/shard_map/all_to_all | solution.py:107
  129.3 0.9 fusion.16
  (47 shorter events, 5.8 us)
Async XLA Ops:
  0.6 25.2 %copy-start = (bf16[2048,128]{1,0:T(8,128)(2,1)S(1)}, bf16[2048,128]{1,0:T(8,128)(2,1)}, u32[]{:S(2)}) copy-start(bf16[2048,128]{1,0:T(8,128)(2,1)} %param.21) | copy-start | bytes 1572868
  28.7 22.7 %copy-start.5 = (f32[128]{0:T(128)S(1)}, f32[128]{0:T(128)}, u32[]{:S(2)}) copy-start(f32[128]{0:T(128)} %param.26) | copy-start | bytes 1540
  30.0 40.0 %copy-start.2 = (bf16[2048,128]{1,0:T(8,128)(2,1)S(1)}, bf16[2048,128]{1,0:T(8,128)(2,1)}, u32[]{:S(2)}) copy-start(bf16[2048,128]{1,0:T(8,128)(2,1)} %param.27) | copy-start | bytes 1572868
  30.7 10.4 %all-to-all-start = ((bf16[4,64,128]{2,0,1:T(4,128)(2,1)}), bf16[4,64,128]{2,0,1:T(4,128)(2,1)S(1)}, u32[]{:S(2)}, u32[]{:S(2)}) async-start(bf16[4,64,128]{2,0,1:T(4,128)(2,1)} %copy.66), calls=%async_computation | async-start | bytes 131072 | tf_op jit(solution)/shard_map/all_to_all | solution.py:73
  41.1 48.1 %copy-start.3 = (bf16[4,2048]{1,0:T(4,128)(2,1)S(1)}, bf16[4,2048]{1,0:T(4,128)(2,1)}, u32[]{:S(2)}) copy-start(bf16[4,2048]{1,0:T(4,128)(2,1)} %param.16) | copy-start | bytes 49156
  41.2 48.2 %copy-start.6 = (f32[2048]{0:T(1024)S(1)}, f32[2048]{0:T(1024)}, u32[]{:S(2)}) copy-start(f32[2048]{0:T(1024)} %param.28) | copy-start | bytes 24580
  45.6 2.0 %copy-start.1 = (f32[4,16,128,128]{3,2,1,0:T(8,128)}, f32[4,16,128,128]{3,2,1,0:T(8,128)S(1)}, u32[]{:S(2)}) copy-start(f32[4,16,128,128]{3,2,1,0:T(8,128)S(1)} %multiply_add_fusion) | copy-start | bytes 12582916
  79.2 10.0 %all-to-all-start.1 = ((bf16[16,4,128]{2,1,0:T(4,128)(2,1)}), bf16[16,4,128]{2,1,0:T(4,128)(2,1)S(1)}, u32[]{:S(2)}, u32[]{:S(2)}) async-start(bf16[16,4,128]{2,1,0:T(4,128)(2,1)} %constant_dynamic-update-slice_fusion), calls=%async_computation.1 | async-start | bytes 32768 | tf_op jit(solution)/shard_map/all_to_all | solution.py:80
  106.9 12.3 %copy-start.7 = (bf16[4,2]{0,1:T(2,128)(2,1)S(1)}, bf16[4,2]{0,1:T(2,128)(2,1)}, u32[]{:S(2)}) copy-start(bf16[4,2]{0,1:T(2,128)(2,1)} %param.19) | copy-start | bytes 52
  106.9 12.3 %copy-start.4 = (s32[4,2]{0,1:T(2,128)S(1)}, s32[4,2]{0,1:T(2,128)}, u32[]{:S(2)}) copy-start(s32[4,2]{0,1:T(2,128)} %param.18) | copy-start | bytes 100
  115.7 13.5 %all-to-all-start.3 = ((bf16[16,3,2048]{2,1,0:T(4,128)(2,1)}), bf16[16,3,2048]{2,1,0:T(4,128)(2,1)S(1)}, u32[]{:S(2)}, u32[]{:S(2)}) async-start(bf16[16,3,2048]{2,1,0:T(4,128)(2,1)} %copy.73), calls=%async_computation.3 | async-start | bytes 524288 | tf_op jit(solution)/shard_map/all_to_all | solution.py:107
